TPU v7x, 32 devices: a whole 2x2x4 slice. The times are simulated.
32 devices in a mesh: sp: 8 (over z, x), dp: 4 (over y, core).
Axes of the slice: x: 2, y: 2, z: 4, core: 2. Of those that a mesh axis runs over, the one named last changes fastest.
Arguments:
- gate_in: bfloat16 [4, 4096, 1024], P('dp', 'sp'), may hold values from -6 to 6
- value_in: bfloat16 [4, 4096, 1024], P('dp', 'sp'), may hold values from -6 to 6
- segments: int32 [4, 4096], P('dp', 'sp'), may hold values from 0 to 1, never falling along the last dimension, each value on 1 to 3072 neighbouring positions
- value_gain: bfloat16 [1024], P('sp'), may hold values from 0.099609375 to 1.8984375
- mixing: bfloat16 [8, 1024, 1024], P('sp', 'dp'), may hold values from -0.1875 to 0.1875
- mixing_bias: bfloat16 [8, 1024], P('sp'), may hold values from 0.099609375 to 1.8984375
Outputs:
- gated: bfloat16 [4, 4096, 1024], P('dp', 'sp')
Inputs may be any that keep to these rules, and one draw needn't show every extreme that they name: `segments`: within each sequence the numbers never fall, every number 0 to 1 occurs, a document spans at most 3072 positions and some document spans exactly that.
All inputs are finite; a program needn't handle non-finite values.
Results may differ from a plain program's by a relative error of at most 0.0054.
Values may be sent and summed in bfloat16 or wider, within the bound.
No kernel may reach another device: no remote copies, remote signals or barrier semaphores. Data moves between devices by JAX's collectives and lax.ppermute only.
A program may use at most 128 MiB of HBM per device.

v0:
```python
import jax
import jax.numpy as jnp
from jax import lax
from jax.sharding import PartitionSpec as P

HEAD_DIM = 128


epsilon = 1e-06


def head_norm(values, gain_f, head_dim):
    shaped = values.reshape(values.shape[:-1] + (values.shape[-1] // head_dim, head_dim))
    scaled = shaped * lax.rsqrt(jnp.mean(shaped * shaped, axis=-1, keepdims=True) + epsilon)
    return (scaled.reshape(values.shape) * gain_f).astype(jnp.bfloat16)


def per_device(gate_in, value_in, segments, value_gain, mixing, mixing_bias):
    sp_count = lax.axis_size("sp")
    sequences = value_in.shape[0]
    tokens = value_in.shape[1]
    length = tokens * sp_count
    block_len = mixing.shape[2]
    heads_here = mixing.shape[0]
    head_dim = HEAD_DIM
    id_tile = jnp.broadcast_to(
        segments.astype(jnp.bfloat16)[:, :, None], (sequences, tokens, sp_count)
    )
    value_heads, id_heads = (
        lax.all_to_all(value_in, "sp", split_axis=2, concat_axis=1, tiled=True),
        lax.all_to_all(id_tile, "sp", split_axis=2, concat_axis=1, tiled=True),
    )
    gain_f = value_gain.astype(jnp.float32)
    normed = head_norm(jax.nn.gelu(value_heads.astype(jnp.float32)), gain_f, head_dim)
    blocks = sequences * length // block_len
    value_blocks = normed.reshape(blocks, block_len, heads_here, head_dim)
    id_blocks = id_heads.reshape(blocks, block_len)
    bias_f = mixing_bias.astype(jnp.float32)
    nothing = jnp.zeros((), jnp.bfloat16)
    shard_piece = lax.all_gather(mixing, "dp", axis=1, tiled=True)
    bias_rows = jnp.transpose(bias_f)[:, :, None]

    def one_block(pair_item):
        block_values, block_ids = pair_item
        same_doc = block_ids[:, None] == block_ids[None, :]
        masked = jnp.where(same_doc[None, :, :], shard_piece, nothing)
        summed = jnp.einsum(
            "hts,shd->thd", masked, block_values, preferred_element_type=jnp.float32
        )
        return (summed + bias_rows).astype(jnp.bfloat16)

    mixed = lax.map(one_block, (value_blocks, id_blocks))
    mixed = mixed.reshape(sequences, length, heads_here * head_dim)
    returned = lax.all_to_all(mixed, "sp", split_axis=1, concat_axis=2, tiled=True)
    return (jax.nn.gelu(gate_in.astype(jnp.float32)) * returned.astype(jnp.float32)).astype(
        jnp.bfloat16
    )


def solution(mesh):
    return jax.shard_map(
        per_device,
        mesh=mesh,
        in_specs=(
            P("dp", "sp", None),
            P("dp", "sp", None),
            P("dp", "sp"),
            P("sp"),
            P("sp", "dp", None),
            P("sp", None),
        ),
        out_specs=P("dp", "sp", None),
        check_vma=False,
    )
```

profile of v0, /device:TPU:0, one launch (start us, length us, event | category | flops | bytes accessed | tf_op | source)
XLA Modules:
  0.0 162.7 jit_solution(6695371021300023633)
XLA Ops:
  6.5 0.7 all-gather.2.cloned.1.call-update
  7.3 0.7 convert_reduce_fusion
  8.0 0.5 broadcast.193
  8.5 0.6 reduce.7
  9.0 0.6 reshape.283
  9.7 7.3 %all-to-all-start.1 = ((bf16[8,2,256]{2,1,0:T(2,128)(2,1)}), bf16[8,2,256]{2,1,0:T(2,128)(2,1)S(1)}, u32[]{:S(2)}, u32[]{:S(2)}) async-start(bf16[8,2,256]{2,1,0:T(2,128)(2,1)} %reshape.283), calls=%async_computation.1 | async-start | bytes 16384 | tf_op jit(solution)/shard_map/all_to_all | solution.py:31
  16.9 4.7 %copy.44 = bf16[1,512,1024]{1,0,2:T(2,128)(2,1)S(1)} copy(bf16[1,512,1024]{2,1,0:T(8,128)(2,1)} %param.9) | data formatting | bytes 2097152 | tf_op args[1]
  21.6 6.9 %reduce.6 = bf16[1024,512]{1,0:T(8,128)(2,1)S(1)} reduce(bf16[1024,1,512]{2,1,0:T(2,128)(2,1)S(1)} %bitcast.83, bf16[]{:T(256)} %broadcast.193), dimensions={1}, to_apply=%bitcast.59.reduce_sub_computation | reduce | bytes 2097154
  28.6 1.6 reshape.281
  30.2 6.0 %all-to-all-start = ((bf16[8,2,32768]{2,1,0:T(2,128)(2,1)}), bf16[8,2,32768]{2,1,0:T(2,128)(2,1)S(1)}, u32[]{:S(2)}, u32[]{:S(2)}) async-start(bf16[8,2,32768]{2,1,0:T(2,128)(2,1)} %reshape.281), calls=%async_computation | async-start | bytes 2097152 | tf_op jit(solution)/shard_map/all_to_all | solution.py:30
  36.3 25.3 %all-to-all-done = bf16[8,2,32768]{2,1,0:T(2,128)(2,1)S(1)} async-done(((bf16[8,2,32768]{2,1,0:T(2,128)(2,1)}), bf16[8,2,32768]{2,1,0:T(2,128)(2,1)S(1)}, u32[]{:S(2)}, u32[]{:S(2)}) %all-to-all-start) | async-done | bytes 1048608 | tf_op jit(solution)/shard_map/all_to_all | solution.py:30
  61.6 1.0 reshape.282
  62.6 0.3 copy.45
  62.9 0.5 copy.46
  63.5 0.8 fusion.47
  64.4 1.7 %fusion.31 = bf16[4,1024,1,128]{3,1,2,0:T(8,128)(2,1)} fusion(f32[4,1024,1,128]{3,1,2,0:T(8,128)S(1)} %bitcast.79, f32[128]{0:T(128)S(1)} %convert_element_type.89, f32[4,1024]{1,0:T(4,128)S(1)} %rsqrt.12), kind=kLoop, calls=%fused_computation.31 | loop fusion | flops 5767168 | bytes 3162624 | tf_op jit(solution)/shard_map/convert_element_type | solution.py:15
  66.0 11.5 %while.10 = (s32[]{:T(128)}, bf16[4,1024,1,128]{3,1,0,2:T(8,128)(2,1)S(1)}, bf16[4,1024,1,128]{3,1,2,0:T(8,128)(2,1)}, bf16[4,1024]{1,0:T(4,128)(2,1)S(1)}, bf16...) while((s32[]{:T(128)}, bf16[4,1024,1,128]{3,1,0,2:T(8,128)(2,1)S(1)}, ...), condition=%wide.region_2.3_spmd, body=%wide.region_1.2_spmd.sunk | while | flops 270794752 | bytes 3682901 | solution.py:52
  66.1 2.6 %fusion.53 = bf16[1,1024,1,128]{1,3,2,0:T(8,128)(2,1)S(1)} fusion(bf16[1,1024,1024]{2,1,0:T(8,128)(2,1)} %get-tuple-element.105, bf16[1024]{0:T(1024)(128)(2,1)S(1)} %dynamic-slice_reduce_fusion.2, f32[1024]{0:T(1024)S(1)} %bitcast.89, bf16[4,1024,1,128]{3,1,2,0:T(8,128)(2,1)} %get-tuple-element.103, s32[]{:T(128)} %get-tuple-element.94), kind=kOutput, calls=%fused_computation.6.clone.1 | convolution fusion | flops 270794752 | bytes 2630144 | tf_op jit(solution)/shard_map/while/body/eval_jaxpr/hts,shd->thd/dot_general | solution.py:47
  69.0 2.6 %fusion.53 = bf16[1,1024,1,128]{1,3,2,0:T(8,128)(2,1)S(1)} fusion(bf16[1,1024,1024]{2,1,0:T(8,128)(2,1)} %get-tuple-element.105, bf16[1024]{0:T(1024)(128)(2,1)S(1)} %dynamic-slice_reduce_fusion.2, f32[1024]{0:T(1024)S(1)} %bitcast.89, bf16[4,1024,1,128]{3,1,2,0:T(8,128)(2,1)} %get-tuple-element.103, s32[]{:T(128)} %get-tuple-element.94), kind=kOutput, calls=%fused_computation.6.clone.1 | convolution fusion | flops 270794752 | bytes 2630144 | tf_op jit(solution)/shard_map/while/body/eval_jaxpr/hts,shd->thd/dot_general | solution.py:47
  71.8 2.6 %fusion.53 = bf16[1,1024,1,128]{1,3,2,0:T(8,128)(2,1)S(1)} fusion(bf16[1,1024,1024]{2,1,0:T(8,128)(2,1)} %get-tuple-element.105, bf16[1024]{0:T(1024)(128)(2,1)S(1)} %dynamic-slice_reduce_fusion.2, f32[1024]{0:T(1024)S(1)} %bitcast.89, bf16[4,1024,1,128]{3,1,2,0:T(8,128)(2,1)} %get-tuple-element.103, s32[]{:T(128)} %get-tuple-element.94), kind=kOutput, calls=%fused_computation.6.clone.1 | convolution fusion | flops 270794752 | bytes 2630144 | tf_op jit(solution)/shard_map/while/body/eval_jaxpr/hts,shd->thd/dot_general | solution.py:47
  74.7 2.6 %fusion.53 = bf16[1,1024,1,128]{1,3,2,0:T(8,128)(2,1)S(1)} fusion(bf16[1,1024,1024]{2,1,0:T(8,128)(2,1)} %get-tuple-element.105, bf16[1024]{0:T(1024)(128)(2,1)S(1)} %dynamic-slice_reduce_fusion.2, f32[1024]{0:T(1024)S(1)} %bitcast.89, bf16[4,1024,1,128]{3,1,2,0:T(8,128)(2,1)} %get-tuple-element.103, s32[]{:T(128)} %get-tuple-element.94), kind=kOutput, calls=%fused_computation.6.clone.1 | convolution fusion | flops 270794752 | bytes 2630144 | tf_op jit(solution)/shard_map/while/body/eval_jaxpr/hts,shd->thd/dot_general | solution.py:47
  77.6 16.7 %copy.63 = bf16[1,4096,128]{2,0,1:T(2,128)(2,1)S(1)} copy(bf16[1,4096,128]{2,1,0:T(8,128)(2,1)S(1)} %bitcast.86) | data formatting | bytes 2097152 | tf_op jit(solution)/shard_map/reshape | solution.py:53
  94.3 22.3 %reduce.8 = bf16[4096,128]{1,0:T(8,128)(2,1)S(1)} reduce(bf16[4096,1,128]{2,1,0:T(2,128)(2,1)S(1)} %bitcast.82, bf16[]{:T(256)} %broadcast.193), dimensions={1}, to_apply=%bitcast.68.reduce_sub_computation | reduce | bytes 2097154
  116.6 1.1 reshape.285
  117.7 3.6 %all-to-all-start.2 = ((bf16[8,2,32768]{2,1,0:T(2,128)(2,1)}), bf16[8,2,32768]{2,1,0:T(2,128)(2,1)S(1)}, u32[]{:S(2)}, u32[]{:S(2)}) async-start(bf16[8,2,32768]{2,1,0:T(2,128)(2,1)} %reshape.285), calls=%async_computation.2 | async-start | bytes 2097152 | tf_op jit(solution)/shard_map/all_to_all | solution.py:54
  121.3 1.3 copy.43
  122.6 24.4 %all-to-all-done.2 = bf16[8,2,32768]{2,1,0:T(2,128)(2,1)S(1)} async-done(((bf16[8,2,32768]{2,1,0:T(2,128)(2,1)}), bf16[8,2,32768]{2,1,0:T(2,128)(2,1)S(1)}, u32[]{:S(2)}, u32[]{:S(2)}) %all-to-all-start.2) | async-done | bytes 1048608 | tf_op jit(solution)/shard_map/all_to_all | solution.py:54
  147.1 1.0 reshape.286
  148.3 1.5 convert_bitcast_fusion
  149.8 2.0 %copy.55 = f32[1,512,8,128]{1,3,2,0:T(8,128)S(1)} copy(f32[1,512,8,128]{3,1,2,0:T(8,128)} %convert_bitcast_fusion) | data formatting | bytes 4194304 | tf_op jit(solution)/shard_map/convert_element_type | solution.py:55
  151.8 1.8 %fusion.46 = bf16[1,512,1024]{1,2,0:T(8,128)(2,1)} fusion(bf16[1,512,1024]{1,2,0:T(8,128)(2,1)S(1)} %copy-done, f32[1,512,8,128]{1,3,2,0:T(8,128)S(1)} %copy.55), kind=kLoop, calls=%fused_computation.46 | loop fusion | flops 5767168 | bytes 4194304 | tf_op jit(solution)/shard_map/convert_element_type | solution.py:55
  153.6 2.3 %copy.56 = bf16[1,512,1024]{2,1,0:T(8,128)(2,1)} copy(bf16[1,512,1024]{1,2,0:T(8,128)(2,1)} %fusion.46) | data formatting | bytes 2097152 | tf_op jit(solution)/shard_map/convert_element_type | solution.py:55
  (35 shorter events, 1.2 us)
Async XLA Ops:
  6.5 59.5 %all-gather.2.cloned.1.call-start = ((), (), s32[]{:S(2)}) async-start(), calls=%async_computation.3 | async-start | bytes 2621440 | tf_op jit(solution)/shard_map/all_gather | solution.py:40
  9.7 20.5 %all-to-all-start.1 = ((bf16[8,2,256]{2,1,0:T(2,128)(2,1)}), bf16[8,2,256]{2,1,0:T(2,128)(2,1)S(1)}, u32[]{:S(2)}, u32[]{:S(2)}) async-start(bf16[8,2,256]{2,1,0:T(2,128)(2,1)} %reshape.283), calls=%async_computation.1 | async-start | bytes 16384 | tf_op jit(solution)/shard_map/all_to_all | solution.py:31
  28.6 7.6 %copy-start.4 = (bf16[128]{0:T(256)(128)(2,1)S(1)}, bf16[128]{0:T(256)(128)(2,1)}, u32[]{:S(2)}) copy-start(bf16[128]{0:T(256)(128)(2,1)} %param.11) | copy-start | bytes 772
  28.6 7.6 %copy-start.3 = (bf16[1,1024]{1,0:T(2,128)(2,1)S(1)}, bf16[1,1024]{1,0:T(2,128)(2,1)}, u32[]{:S(2)}) copy-start(bf16[1,1024]{1,0:T(2,128)(2,1)} %param.13) | copy-start | bytes 6148
  30.2 31.4 %all-to-all-start = ((bf16[8,2,32768]{2,1,0:T(2,128)(2,1)}), bf16[8,2,32768]{2,1,0:T(2,128)(2,1)S(1)}, u32[]{:S(2)}, u32[]{:S(2)}) async-start(bf16[8,2,32768]{2,1,0:T(2,128)(2,1)} %reshape.281), calls=%async_computation | async-start | bytes 2097152 | tf_op jit(solution)/shard_map/all_to_all | solution.py:30
  64.3 1.7 %copy-start.1 = (bf16[4,1024,1,128]{3,1,0,2:T(8,128)(2,1)S(1)}, bf16[4,1024,1,128]{3,1,0,2:T(8,128)(2,1)}, u32[]{:S(2)}) copy-start(bf16[4,1024,1,128]{3,1,0,2:T(8,128)(2,1)} %custom-call) | copy-start | bytes 3145732
  116.6 4.7 %copy-start.2 = (bf16[1,512,1024]{2,1,0:T(8,128)(2,1)S(1)}, bf16[1,512,1024]{2,1,0:T(8,128)(2,1)}, u32[]{:S(2)}) copy-start(bf16[1,512,1024]{2,1,0:T(8,128)(2,1)} %param.8) | copy-start | bytes 3145732
  117.7 29.3 %all-to-all-start.2 = ((bf16[8,2,32768]{2,1,0:T(2,128)(2,1)}), bf16[8,2,32768]{2,1,0:T(2,128)(2,1)S(1)}, u32[]{:S(2)}, u32[]{:S(2)}) async-start(bf16[8,2,32768]{2,1,0:T(2,128)(2,1)} %reshape.285), calls=%async_computation.2 | async-start | bytes 2097152 | tf_op jit(solution)/shard_map/all_to_all | solution.py:54
  149.8 2.0 %copy-start = (bf16[1,512,1024]{1,2,0:T(8,128)(2,1)S(1)}, bf16[1,512,1024]{1,2,0:T(8,128)(2,1)}, u32[]{:S(2)}) copy-start(bf16[1,512,1024]{1,2,0:T(8,128)(2,1)} %copy.43) | copy-start | bytes 3145732
Sparse Core Ops, SparseCore 0:
  8.9 25.2 all-gather.1
where the time goes:
time: 163 us
  waiting for transfers between devices  50.5 us (31%)
  other arithmetic  36.3 us (22%)
  local copies, waits for them, and re-layouts  34.9 us (21%)
  starting transfers between devices  16.8 us (10%)
  between operations  13.6 us (8%)
  matrix products  10.4 us (6%)
    unnamed x3, other arithmetic  29.8 us
    all_to_all x1, waiting for transfers between devices, per_device(): lax.all_to_all(value_in, 'sp', split_axis=2, concat_axis=1, tiled=True)  25.3 us
    all_to_all x1, waiting for transfers between devices, per_device(): lax.all_to_all(mixed, 'sp', split_axis=1, concat_axis=2, tiled=True)  24.4 us
    reshape x1, local copies, waits for them, and re-layouts, per_device(): mixed = mixed.reshape(sequences, length, heads_here * head_dim)  16.7 us
    unnamed x21, local copies, waits for them, and re-layouts  11.9 us
    dot_general x4, matrix products, one_block(): jnp.einsum('hts,shd->thd', masked, block_values, preferred_element_type=j...  10.4 us
    all_to_all x1, starting transfers between devices, per_device(): lax.all_to_all(id_tile, 'sp', split_axis=2, concat_axis=1, tiled=True)  7.28 us
    all_to_all x1, starting transfers between devices, per_device(): lax.all_to_all(value_in, 'sp', split_axis=2, concat_axis=1, tiled=True)  5.99 us
  transfers between devices with their start and end apart: 4, of which 2 were waited for; matrix products, arithmetic and copies ran while one was open for 13% of the time, Pallas kernels for 0%

commit v1 on v0

v1 whole, which is shorter than its diff:
```python
import functools

import jax
import jax.numpy as jnp
from jax import lax
from jax.experimental import pallas as pl
from jax.experimental.pallas import tpu as pltpu
from jax.sharding import PartitionSpec as P

HEAD_DIM = 128
LANES = 128
ID_ROWS = 16

epsilon = 1e-06


def pack_kernel(seg_ref, value_ref, out_ref):
    tokens = value_ref.shape[0]
    act = jax.nn.gelu(value_ref[...].astype(jnp.float32))
    scaled = act * lax.rsqrt(jnp.mean(act * act, axis=-1, keepdims=True) + epsilon)
    out_ref[0, :tokens, :] = scaled.astype(jnp.bfloat16)
    ids = seg_ref[...].astype(jnp.float32)
    rows = [ids[:, i * LANES:(i + 1) * LANES] for i in range(tokens // LANES)]
    rows.append(jnp.zeros((ID_ROWS - len(rows), LANES), jnp.float32))
    out_ref[0, tokens:, :] = jnp.concatenate(rows, axis=0).astype(jnp.bfloat16)


def pack(segments, values):
    tokens, width = values.shape
    heads = width // HEAD_DIM
    return pl.pallas_call(
        pack_kernel,
        grid=(heads,),
        in_specs=[
            pl.BlockSpec((1, tokens), lambda h: (0, 0)),
            pl.BlockSpec((tokens, HEAD_DIM), lambda h: (0, h)),
        ],
        out_specs=pl.BlockSpec((1, tokens + ID_ROWS, HEAD_DIM), lambda h: (h, 0, 0)),
        out_shape=jax.ShapeDtypeStruct((heads, tokens + ID_ROWS, HEAD_DIM), jnp.bfloat16),
        name="pack",
    )(segments, values)


def column(row):
    return jnp.broadcast_to(row, (LANES, LANES)).T


def mix_kernel(pos_ref, recv_ref, gain_ref, bias_ref, *rest, tokens, count):
    pieces, (out_ref, m_ref, ids_ref, biasc_ref, v_ref, sems) = rest[:count], rest[count:]
    blocks, block_len, _ = out_ref.shape
    shards = block_len // tokens
    rows = block_len // count

    def copy(i):
        start = pl.multiple_of(pos_ref[i] * rows, rows)
        return pltpu.make_async_copy(pieces[i].at[0], m_ref.at[pl.ds(start, rows)], sems.at[i])

    for i in range(count):
        copy(i).start()
    gain = gain_ref[...].astype(jnp.float32)
    for c in range(block_len // LANES):
        biasc_ref[c * LANES:(c + 1) * LANES, :] = column(
            bias_ref[:, c * LANES:(c + 1) * LANES].astype(jnp.float32)
        )
    for i in range(count):
        copy(i).wait()

    for q in range(blocks):
        lows, highs = [], []
        for j in range(shards):
            tile = recv_ref[q * shards + j, tokens:, :].astype(jnp.float32)
            used = tile[:tokens // LANES]
            lows.append(jnp.min(used))
            highs.append(jnp.max(used))
            for i in range(tokens // LANES):
                base = j * tokens + i * LANES
                ids_ref[base:base + LANES, :] = column(tile[i:i + 1])
        low = functools.reduce(jnp.minimum, lows).astype(jnp.int32)
        high = functools.reduce(jnp.maximum, highs).astype(jnp.int32)

        def part(doc):
            here = ids_ref[...] == doc.astype(jnp.float32)
            for j in range(shards):
                at = slice(j * tokens, (j + 1) * tokens)
                values = recv_ref[q * shards + j, :tokens, :].astype(jnp.float32)
                v_ref[at, :] = jnp.where(here[at], values, 0.0).astype(jnp.bfloat16)
            summed = jnp.dot(m_ref[...], v_ref[...], preferred_element_type=jnp.float32)
            return here, summed * gain + biasc_ref[...]

        out_ref[q] = part(low)[1].astype(jnp.bfloat16)

        def more(doc, _):
            here, result = part(doc)
            old = out_ref[q].astype(jnp.float32)
            out_ref[q] = jnp.where(here, result, old).astype(jnp.bfloat16)
            return 0

        lax.fori_loop(low + 1, high + 1, more, 0)


def mix(positions, recv, gain, bias, pieces, tokens):
    count = len(pieces)
    block_len = pieces[0].shape[2]
    blocks = recv.shape[0] * tokens // block_len
    vmem = pl.BlockSpec(memory_space=pltpu.VMEM)
    return pl.pallas_call(
        functools.partial(mix_kernel, tokens=tokens, count=count),
        in_specs=[pl.BlockSpec(memory_space=pltpu.SMEM), vmem, vmem, vmem]
        + [pl.BlockSpec(memory_space=pl.ANY)] * count,
        out_specs=vmem,
        out_shape=jax.ShapeDtypeStruct((blocks, block_len, HEAD_DIM), jnp.bfloat16),
        scratch_shapes=[
            pltpu.VMEM((block_len, block_len), jnp.bfloat16),
            pltpu.VMEM((block_len, HEAD_DIM), jnp.float32),
            pltpu.VMEM((block_len, HEAD_DIM), jnp.float32),
            pltpu.VMEM((block_len, HEAD_DIM), jnp.bfloat16),
            pltpu.SemaphoreType.DMA((count,)),
        ],
        name="mix",
    )(positions, recv, gain, bias, *pieces)


def gate_kernel(gate_ref, mixed_ref, out_ref):
    gate = jax.nn.gelu(gate_ref[...].astype(jnp.float32))
    out_ref[...] = (gate * mixed_ref[0].astype(jnp.float32)).astype(jnp.bfloat16)


def apply_gate(gate_in, mixed):
    heads, tokens, head_dim = mixed.shape
    spec = pl.BlockSpec((tokens, head_dim), lambda h: (0, h))
    return pl.pallas_call(
        gate_kernel,
        grid=(heads,),
        in_specs=[spec, pl.BlockSpec((1, tokens, head_dim), lambda h: (h, 0, 0))],
        out_specs=spec,
        out_shape=jax.ShapeDtypeStruct(gate_in.shape, jnp.bfloat16),
        name="gate",
    )(gate_in, mixed)


def gather_rows(mixing):
    n = lax.axis_size("dp")
    me = lax.axis_index("dp")
    pieces, places = [], []
    for step in range(0, n, 2):
        piece = mixing
        if step:
            piece = lax.ppermute(mixing, "dp", [(i, (i + step) % n) for i in range(n)])
        other = lax.ppermute(piece, "dp", [(i, i ^ 1) for i in range(n)])
        place = (me + n - step) % n
        pieces += [piece, other]
        places += [place, place ^ 1]
    return pieces, jnp.stack(places).astype(jnp.int32)


def per_device(gate_in, value_in, segments, value_gain, mixing, mixing_bias):
    tokens = value_in.shape[1]
    pieces, places = gather_rows(mixing)
    packed = pack(segments, value_in[0])
    recv = lax.all_to_all(packed, "sp", split_axis=0, concat_axis=0, tiled=True)
    mixed = mix(places, recv, value_gain[None, :], mixing_bias, pieces, tokens)
    mixed = mixed.reshape(-1, tokens, HEAD_DIM)
    returned = lax.all_to_all(mixed, "sp", split_axis=0, concat_axis=0, tiled=True)
    return apply_gate(gate_in[0], returned)[None]


def solution(mesh):
    return jax.shard_map(
        per_device,
        mesh=mesh,
        in_specs=(
            P("dp", "sp", None),
            P("dp", "sp", None),
            P("dp", "sp"),
            P("sp"),
            P("sp", "dp", None),
            P("sp", None),
        ),
        out_specs=P("dp", "sp", None),
        check_vma=False,
    )
```

time: 163 us -> 85 us (0.52)
  other arithmetic: 36.3 us -> 0.69 us
  local copies, waits for them, and re-layouts: 34.9 us -> 0.98 us
  blocking collectives: 0 us -> 29.7 us
  waiting for transfers between devices: 50.5 us -> 24.2 us
  Pallas kernels: 0 us -> 19.9 us
  between operations: 13.6 us -> 0.03 us
  matrix products: 10.4 us -> 0 us
  starting transfers between devices: 16.8 us -> 9 us
    all_to_all x3 -> x1, waiting for transfers between devices: 49.8 us -> 11.1 us  [per_device(): recv = lax.all_to_all(packed, 'sp', split_axis=0, concat_axis=0, tiled=True)]
    unnamed x3 -> x0, other arithmetic: 29.8 us -> none
    all_to_all x0 -> x1, blocking collectives: none -> 29.7 us  [per_device(): lax.all_to_all(mixed, 'sp', split_axis=0, concat_axis=0, tiled=True)]
    pallas_call x0 -> x3, Pallas kernels: none -> 19.9 us  [the longest x1 8.14 us: mix(): pl.pallas_call(functools.partial(mix_kernel, tokens=tokens, count=count),...]
    reshape x2 -> x0, local copies, waits for them, and re-layouts: 16.8 us -> none  [the longest x1 16.7 us: per_device(): mixed = mixed.reshape(sequences, length, heads_here * head_dim)]
    ppermute x0 -> x3, waiting for transfers between devices: none -> 13.1 us  [the longest x1 11.9 us: gather_rows(): piece = lax.ppermute(mixing, 'dp', [(i, (i + step) % n) for i in range(n)])]
    unnamed x21 -> x10, local copies, waits for them, and re-layouts: 11.9 us -> 0.98 us
    dot_general x4 -> x0, matrix products: 10.4 us -> none  [one_block(): jnp.einsum('hts,shd->thd', masked, block_values, preferred_element_type=j...]
  transfers between devices with their start and end apart: 4 -> 4, of which waited for: 2 -> 3; matrix products, arithmetic and copies ran while one was open for 13% -> 1% of each run, Pallas kernels for 0% -> 0%
where the time goes in v1:
time: 85 us; the launch traced here: 84.5 us
  blocking collectives  29.7 us (35%)
  waiting for transfers between devices  24.2 us (28%)
  Pallas kernels  19.9 us (23%)
  starting transfers between devices  9 us (11%)
  local copies, waits for them, and re-layouts  0.98 us (1%)
    all_to_all x1, blocking collectives, per_device(): lax.all_to_all(mixed, 'sp', split_axis=0, concat_axis=0, tiled=True)  29.7 us
    ppermute x1, waiting for transfers between devices, gather_rows(): piece = lax.ppermute(mixing, 'dp', [(i, (i + step) % n) for i in range(n)])  11.9 us
    all_to_all x1, waiting for transfers between devices, per_device(): recv = lax.all_to_all(packed, 'sp', split_axis=0, concat_axis=0, tiled=True)  11.1 us
    pallas_call x1, Pallas kernels, mix(): pl.pallas_call(functools.partial(mix_kernel, tokens=tokens, count=count),...  8.14 us
    all_to_all x1, starting transfers between devices, per_device(): recv = lax.all_to_all(packed, 'sp', split_axis=0, concat_axis=0, tiled=True)  7.41 us
    pallas_call x1, Pallas kernels, apply_gate(): pl.pallas_call(gate_kernel, grid=(heads,), in_specs=[spec, pl.BlockSpec((...  5.88 us
    pallas_call x1, Pallas kernels, pack(): pl.pallas_call(pack_kernel, grid=(heads,), in_specs=[pl.BlockSpec((1, tok...  5.84 us
  transfers between devices with their start and end apart: 4, of which 3 were waited for; matrix products, arithmetic and copies ran while one was open for 1% of the time, Pallas kernels for 0%

profile of v1, /device:TPU:0, one launch (start us, length us, event | category | flops | bytes accessed | tf_op | source)
XLA Modules:
  0.0 84.5 jit_solution(17391938065985687172)
XLA Ops:
  0.0 5.8 %pack.1 = bf16[8,528,128]{2,1,0:T(8,128)(2,1)} custom-call(s32[1,512]{1,0:T(1,128)} %seg_ref.1, bf16[512,1024]{1,0:T(8,128)(2,1)} %bitcast.11), custom_call_target="tpu_custom_call" | custom-call | tf_op jit(solution)/shard_map/pack/pallas_call | solution.py:31
  5.8 0.0 copy-start.1
  5.8 7.4 %all-to-all-start = ((bf16[8,528,128]{2,1,0:T(8,128)(2,1)}), bf16[8,528,128]{2,1,0:T(8,128)(2,1)S(1)}, u32[]{:S(2)}, u32[]{:S(2)}) async-start(bf16[8,528,128]{2,1,0:T(8,128)(2,1)} %pack.1), calls=%async_computation | async-start | bytes 2162688 | tf_op jit(solution)/shard_map/all_to_all | solution.py:160
  13.3 0.0 copy-done.1
  13.3 1.6 %collective-permute-start.1 = (bf16[1,256,1024]{2,1,0:T(8,128)(2,1)S(1)}, bf16[1,256,1024]{2,1,0:T(8,128)(2,1)S(1)}, u32[]{:S(2)}, u32[]{:S(2)}) collective-permute-start(bf16[1,256,1024]{2,1,0:T(8,128)(2,1)S(1)} %copy-done.1), channel_id=1, source_target_pairs={{0,2},{1,3},{2,0},{3,1},{4,6},{5,7},{6,4},{7,5},{8,10},{9,11},{10,... | collective-permute-start | bytes 1572872 | tf_op jit(solution)/shard_map/ppermute | solution.py:148
  14.8 0.0 collective-permute-start
  14.8 11.9 %collective-permute-done.1.rest_2_ = bf16[1,256,1024]{2,1,0:T(8,128)(2,1)S(1)} collective-permute-done((bf16[1,256,1024]{2,1,0:T(8,128)(2,1)S(1)}, bf16[1,256,1024]{2,1,0:T(8,128)(2,1)S(1)}, u32[]{:S(2)}, u32[]{:S(2)}) %collective-permute-start.1) | collective-permute-done | bytes 524320 | tf_op jit(solution)/shard_map/ppermute | solution.py:148
  26.7 0.0 copy-start.2
  26.7 0.0 collective-permute-start.2
  26.7 0.7 pad_add_fusion.pos_ref
  27.4 0.0 collective-permute-done.rest_1_
  27.4 0.0 copy-start.3
  27.4 1.2 %collective-permute-done.2.rest_3_ = bf16[1,256,1024]{2,1,0:T(8,128)(2,1)S(1)} collective-permute-done((bf16[1,256,1024]{2,1,0:T(8,128)(2,1)S(1)}, bf16[1,256,1024]{2,1,0:T(8,128)(2,1)S(1)}, u32[]{:S(2)}, u32[]{:S(2)}) %collective-permute-start.2) | collective-permute-done | bytes 524320 | tf_op jit(solution)/shard_map/ppermute | solution.py:149
  28.6 0.0 copy-start.4
  28.6 11.1 %all-to-all-done.recv_ref = bf16[8,528,128]{2,1,0:T(8,128)(2,1)S(1)} async-done(((bf16[8,528,128]{2,1,0:T(8,128)(2,1)}), bf16[8,528,128]{2,1,0:T(8,128)(2,1)S(1)}, u32[]{:S(2)}, u32[]{:S(2)}) %all-to-all-start) | async-done | bytes 1081376 | tf_op jit(solution)/shard_map/all_to_all | solution.py:160
  39.7 0.0 copy-start
  39.7 0.0 copy-done.2
  39.7 0.0 copy-done.3
  39.7 0.0 copy-done.4
  39.7 1.0 %copy-done = bf16[8,528,128]{2,1,0:T(8,128)(2,1)} copy-done((bf16[8,528,128]{2,1,0:T(8,128)(2,1)}, bf16[8,528,128]{2,1,0:T(8,128)(2,1)S(1)}, u32[]{:S(2)}) %copy-start) | copy-done | bytes 1081368
  40.7 8.1 %mix.1 = bf16[4,1024,128]{2,1,0:T(8,128)(2,1)} custom-call(s32[4]{0:T(128)} %pad_add_fusion.pos_ref, bf16[8,528,128]{2,1,0:T(8,128)(2,1)} %copy-done, bf16[1,128]{1,0:T(2,128)(2,1)} %bitcast.12, bf16[1,1024]{1,0:T(2,128)(2,1)} %bias_ref.1, bf16[1,256,1024]{2,1,0:T(8,128)(2,1)} %rest_0_.1, bf16[1,256,1024]{2,1,0:T(8,128)(2,1)} %copy-done.3, ...), custom_call_target="tpu_custom_call" | custom-call | tf_op jit(solution)/shard_map/mix/pallas_call | solution.py:106
  48.8 29.7 %all_to_all.10.mixed_ref = bf16[8,512,128]{2,1,0:T(8,128)(2,1)} all-to-all(bf16[8,512,128]{2,1,0:T(8,128)(2,1)} %bitcast.9), channel_id=1, replica_groups=mesh['sp'=8,'dp'=4] {'sp'}, dimensions={0} | all-to-all | bytes 2097152 | tf_op jit(solution)/shard_map/all_to_all | solution.py:163
  78.6 5.9 %gate.1 = bf16[512,1024]{1,0:T(8,128)(2,1)} custom-call(bf16[512,1024]{1,0:T(8,128)(2,1)} %bitcast.10, bf16[8,512,128]{2,1,0:T(8,128)(2,1)} %all_to_all.10.mixed_ref), custom_call_target="tpu_custom_call" | custom-call | tf_op jit(solution)/shard_map/gate/pallas_call | solution.py:131
Async XLA Ops:
  5.8 7.4 %copy-start.1 = (bf16[1,256,1024]{2,1,0:T(8,128)(2,1)S(1)}, bf16[1,256,1024]{2,1,0:T(8,128)(2,1)}, u32[]{:S(2)}) copy-start(bf16[1,256,1024]{2,1,0:T(8,128)(2,1)} %rest_0_.1) | copy-start | bytes 1572868
  5.8 33.9 %all-to-all-start = ((bf16[8,528,128]{2,1,0:T(8,128)(2,1)}), bf16[8,528,128]{2,1,0:T(8,128)(2,1)S(1)}, u32[]{:S(2)}, u32[]{:S(2)}) async-start(bf16[8,528,128]{2,1,0:T(8,128)(2,1)} %pack.1), calls=%async_computation | async-start | bytes 2162688 | tf_op jit(solution)/shard_map/all_to_all | solution.py:160
  13.3 13.4 %collective-permute-start.1 = (bf16[1,256,1024]{2,1,0:T(8,128)(2,1)S(1)}, bf16[1,256,1024]{2,1,0:T(8,128)(2,1)S(1)}, u32[]{:S(2)}, u32[]{:S(2)}) collective-permute-start(bf16[1,256,1024]{2,1,0:T(8,128)(2,1)S(1)} %copy-done.1), channel_id=1, source_target_pairs={{0,2},{1,3},{2,0},{3,1},{4,6},{5,7},{6,4},{7,5},{8,10},{9,11},{10,... | collective-permute-start | bytes 1572872 | tf_op jit(solution)/shard_map/ppermute | solution.py:148
  14.8 12.6 %collective-permute-start = (bf16[1,256,1024]{2,1,0:T(8,128)(2,1)S(1)}, bf16[1,256,1024]{2,1,0:T(8,128)(2,1)S(1)}, u32[]{:S(2)}, u32[]{:S(2)}) collective-permute-start(bf16[1,256,1024]{2,1,0:T(8,128)(2,1)S(1)} %copy-done.1), channel_id=1, source_target_pairs={{0,1},{1,0},{2,3},{3,2},{4,5},{5,4},{6,7},{7,6},{8,9},{9,8},{10,11... | collective-permute-start | bytes 1572872 | tf_op jit(solution)/shard_map/ppermute | solution.py:149
  26.7 13.0 %copy-start.2 = (bf16[1,256,1024]{2,1,0:T(8,128)(2,1)}, bf16[1,256,1024]{2,1,0:T(8,128)(2,1)S(1)}, u32[]{:S(2)}) copy-start(bf16[1,256,1024]{2,1,0:T(8,128)(2,1)S(1)} %collective-permute-done.1.rest_2_) | copy-start | bytes 1572868
  26.7 1.9 %collective-permute-start.2 = (bf16[1,256,1024]{2,1,0:T(8,128)(2,1)S(1)}, bf16[1,256,1024]{2,1,0:T(8,128)(2,1)S(1)}, u32[]{:S(2)}, u32[]{:S(2)}) collective-permute-start(bf16[1,256,1024]{2,1,0:T(8,128)(2,1)S(1)} %collective-permute-done.1.rest_2_), channel_id=1, source_target_pairs={{0,1},{1,0},{2,3},{3,2},{4,5},{5,4},{6,7},{7,6},{8,9},{9,8},{10,11... | collective-permute-start | bytes 1572872 | tf_op jit(solution)/shard_map/ppermute | solution.py:149
  27.4 12.3 %copy-start.3 = (bf16[1,256,1024]{2,1,0:T(8,128)(2,1)}, bf16[1,256,1024]{2,1,0:T(8,128)(2,1)S(1)}, u32[]{:S(2)}) copy-start(bf16[1,256,1024]{2,1,0:T(8,128)(2,1)S(1)} %collective-permute-done.rest_1_) | copy-start | bytes 1572868
  28.6 11.1 %copy-start.4 = (bf16[1,256,1024]{2,1,0:T(8,128)(2,1)}, bf16[1,256,1024]{2,1,0:T(8,128)(2,1)S(1)}, u32[]{:S(2)}) copy-start(bf16[1,256,1024]{2,1,0:T(8,128)(2,1)S(1)} %collective-permute-done.2.rest_3_) | copy-start | bytes 1572868
  39.7 1.0 %copy-start = (bf16[8,528,128]{2,1,0:T(8,128)(2,1)}, bf16[8,528,128]{2,1,0:T(8,128)(2,1)S(1)}, u32[]{:S(2)}) copy-start(bf16[8,528,128]{2,1,0:T(8,128)(2,1)S(1)} %all-to-all-done.recv_ref) | copy-start | bytes 3244036
